TPU v7x, 32 devices: a whole 2x2x4 slice. The times are simulated.
32 devices in a mesh: grp: 2 (over y), ep: 4 (over z), tp: 4 (over x, core).
Axes of the slice: x: 2, y: 2, z: 4, core: 2. Of those that a mesh axis runs over, the one named last changes fastest.
Arguments:
- mixer_input: bfloat16 [4096, 2048], P(('grp', 'ep', 'tp')), parts along dimension 0, may hold values from -8 to 8
- forget_cumsum: float32 [8, 4096], P('tp', 'grp'), parts along dimension 1, may hold values from -259 to 0, as said below
- mixer_gain: float32 [2048], replicated, may hold values from 0.1 to 1.9
- query_weight: bfloat16 [2048, 1024], P(None, 'tp'), may hold values from -6 to 6
- key_weight: bfloat16 [2048, 1024], P(None, 'tp'), may hold values from -6 to 6
- value_weight: bfloat16 [2048, 1024], P(None, 'tp'), may hold values from -0.125 to 0.125
- out_weight: bfloat16 [1024, 2048], P('tp'), may hold values from -0.1875 to 0.1875
- post_gain: float32 [2048], replicated, may hold values from 0.1 to 1.9
- expert_input: bfloat16 [4096, 2048], P(('grp', 'ep', 'tp')), parts along dimension 0, may hold values from -6 to 6
- expert_gain: float32 [2048], replicated, may hold values from 0.1 to 1.9
- routes: int32 [4096, 2], P(('grp', 'ep', 'tp')), parts along dimension 0, may hold values from 0 to 3, all different within a row; in each aligned block of 128 rows (0 to 127, 128 to 255, ...) at most 72 rows name the same one
- route_weight: float32 [4096, 2], P(('grp', 'ep', 'tp')), parts along dimension 0, may hold values from 0.2 to 1
- expert_gate: bfloat16 [4, 2048, 2048], P('ep', None, 'tp'), may hold values from -0.125 to 0.125
- expert_upward: bfloat16 [4, 2048, 2048], P('ep', None, 'tp'), may hold values from -0.125 to 0.125
- expert_down: bfloat16 [4, 2048, 2048], P('ep', 'tp'), may hold values from -0.125 to 0.125
Outputs:
- mixer_output: bfloat16 [4096, 2048], P(('grp', 'ep', 'tp')), parts along dimension 0
- expert_output: bfloat16 [4096, 2048], P(('grp', 'ep', 'tp')), parts along dimension 0
There are 2 independent parts, one for each index of `grp`. A program takes and returns all parts, laid end to end along the dimension named above; an argument that names none is the same for every part. Nothing has to cross between parts.
Inputs may be any that keep to these rules, and one draw needn't show every extreme that they name: `forget_cumsum`: each head's row never rises along positions. `routes`: A row names 2 different experts. Within the rows of one device (aligned blocks of 128 rows) no expert is named by more than 72 rows, and in every draw some expert is named by exactly 72 rows of some block.
All inputs are finite; a program needn't handle non-finite values.
Results may differ from a plain program's by a relative error of at most 0.012.
Values may be sent and summed in bfloat16 or wider, within the bound.
A program may use at most 128 MiB of HBM per device.

v0:
```python
import functools

import jax
import jax.numpy as jnp
from jax import lax
from jax.experimental import pallas as pl
from jax.experimental.pallas import tpu as pltpu
from jax.sharding import PartitionSpec as P

EPS = 1e-06
MASKED = -1e30
MESH = pl.DeviceIdType.MESH
F32 = jnp.float32
BF16 = jnp.bfloat16


def normalize(row_block, gain):
    values = row_block.astype(F32)
    inverse = lax.rsqrt(jnp.mean(values * values, axis=-1, keepdims=True) + EPS)
    return values * inverse * gain


def tile_of(width, largest):
    return largest if width % largest == 0 else width


def kernel(
    n_ep,
    head_dim,
    normed_ref,
    outgoing_ref,
    query_gate_ref,
    gate_ref,
    post_gain_ref,
    wq_hbm,
    wk_hbm,
    wv_hbm,
    wo_hbm,
    eg_hbm,
    eu_hbm,
    ed_hbm,
    mixer_ref,
    returned_ref,
    wq,
    wk,
    wv,
    wo,
    eg,
    eu,
    ed,
    seg,
    queries,
    kv,
    rows,
    hid,
    res,
    drec,
    erec,
    fin,
    run_max,
    run_sum,
    run_acc,
    attended,
    mdrec,
    merec,
    w_sem,
    ns,
    nr,
    as_,
    ar,
    bs,
    br,
    cs,
    cr,
    ds,
    dr,
    es,
    er,
    fs,
    fr,
    ks,
    kr,
    ms,
    mr,
):
    me = lax.axis_index("ep")
    t = lax.axis_index("tp")
    hi = t // 2
    lo = t % 2
    lo_peer = 2 * hi + (1 - lo)
    hi_peer = 2 * (1 - hi) + lo
    other_hi = 1 - hi
    mix_rows, width = normed_ref.shape
    head_width = wq.shape[1]
    heads = head_width // head_dim
    span = 4 * mix_rows
    cap = outgoing_ref.shape[1]

    def remote(src, dst, send_sem, recv_sem, where):
        return pltpu.make_async_remote_copy(
            src_ref=src,
            dst_ref=dst,
            send_sem=send_sem,
            recv_sem=recv_sem,
            device_id=where,
            device_id_type=MESH,
        )

    loads = [
        pltpu.make_async_copy(src, dst, w_sem.at[i])
        for i, (src, dst) in enumerate(
            ((wq_hbm, wq), (wk_hbm, wk), (wv_hbm, wv), (wo_hbm, wo), (eg_hbm, eg), (eu_hbm, eu), (ed_hbm, ed))
        )
    ]
    barrier = pltpu.get_barrier_semaphore()
    pl.semaphore_signal(barrier, inc=1, device_id={"tp": lo_peer}, device_id_type=MESH)
    pl.semaphore_signal(barrier, inc=1, device_id={"tp": hi_peer}, device_id_type=MESH)

    @pl.loop(1, n_ep)
    def _(j):
        pl.semaphore_signal(barrier, inc=1, device_id={"ep": lax.rem(me + j, n_ep)}, device_id_type=MESH)

    for load in loads:
        load.start()
    pl.semaphore_wait(barrier, 2 + n_ep - 1)

    n_hi = remote(normed_ref, seg.at[t], ns.at[0], nr.at[0], {"tp": hi_peer})
    n_lo = remote(normed_ref, seg.at[t], ns.at[1], nr.at[1], {"tp": lo_peer})
    n_relay = remote(seg.at[hi_peer], seg.at[hi_peer], ns.at[2], nr.at[2], {"tp": lo_peer})
    n_hi.start()
    n_lo.start()

    def copy_a(j):
        to = lax.rem(me - j + n_ep, n_ep)
        return remote(outgoing_ref.at[to], rows.at[j, t], as_.at[j], ar.at[j], {"ep": to})

    def copy_b_hi(j, src):
        return remote(src, rows.at[j, t], bs.at[0, j], br.at[0, j], {"tp": hi_peer})

    def copy_b_lo(j, src):
        return remote(src, rows.at[j, t], bs.at[1, j], br.at[1, j], {"tp": lo_peer})

    def copy_c(j):
        return remote(rows.at[j, hi_peer], rows.at[j, hi_peer], cs.at[j], cr.at[j], {"tp": lo_peer})

    def copy_d(j, h):
        return remote(res.at[j, 2 * h + (1 - lo)], drec.at[j, h], ds.at[h, j], dr.at[h, j], {"tp": lo_peer})

    def copy_e(j):
        return remote(drec.at[j, other_hi], erec.at[j], es.at[j], er.at[j], {"tp": hi_peer})

    def copy_f(j):
        to = lax.rem(me + j, n_ep)
        return remote(fin.at[j], returned_ref.at[me], fs.at[j], fr.at[j], {"ep": to})

    def copy_kv(b):
        return remote(kv.at[b], kv.at[b], ks.at[b], kr.at[b], {"ep": lax.rem(me + 1, n_ep)})

    @pl.loop(1, n_ep)
    def _(j):
        copy_a(j).start()

    copy_b_hi(0, outgoing_ref.at[me]).start()
    copy_b_lo(0, outgoing_ref.at[me]).start()
    seg[t] = normed_ref[...]
    rows[0, t] = outgoing_ref[me]

    n_hi.wait_recv()
    n_relay.start()
    for load in loads[:3]:
        load.wait()
    if n_ep > 1:
        copy_a(1).wait_recv()
        copy_b_hi(1, rows.at[1, t]).start()
        copy_b_lo(1, rows.at[1, t]).start()
    n_lo.wait_recv()
    n_relay.wait_recv()

    @pl.loop(0, 2)
    def _(i):
        x = seg[pl.ds(2 * i, 2)].reshape(2 * mix_rows, width)
        r = pl.ds(pl.multiple_of(i * 2 * mix_rows, 2 * mix_rows), 2 * mix_rows)
        kv[me, r, pl.ds(0, head_width)] = jnp.dot(x, wk[...], preferred_element_type=F32).astype(BF16)
        kv[me, r, pl.ds(head_width, head_width)] = jnp.dot(x, wv[...], preferred_element_type=F32).astype(BF16)
        queries[r, :] = jnp.dot(x, wq[...], preferred_element_type=F32).astype(BF16)

    @pl.when(me + 1 < n_ep)
    def _():
        copy_kv(me).start()

    copy_b_hi(0, outgoing_ref.at[me]).wait_recv()
    copy_c(0).start()
    for load in loads[4:]:
        load.wait()

    f_width = eg.shape[1]
    f_tile = tile_of(f_width, 256)
    d_tile = tile_of(width, 512)

    def step_e(j):
        copy_d(j, 0).wait_recv()
        copy_d(j, 1).wait_recv()
        drec[j, other_hi] = (res[j, hi_peer].astype(F32) + drec[j, other_hi].astype(F32)).astype(BF16)
        copy_e(j).start()

    def step_f(j):
        copy_e(j).wait_recv()
        total = (res[j, t].astype(F32) + drec[j, hi].astype(F32) + erec[j].astype(F32)).astype(BF16)

        @pl.when(j == 0)
        def _():
            returned_ref[me] = total

        @pl.when(j > 0)
        def _():
            fin[j] = total
            copy_f(j).start()

    @pl.loop(0, n_ep)
    def _(j):
        @pl.when(j + 2 < n_ep)
        def _():
            copy_a(j + 2).wait_recv()
            copy_b_hi(j + 2, rows.at[j + 2, t]).start()
            copy_b_lo(j + 2, rows.at[j + 2, t]).start()

        @pl.when(j + 1 < n_ep)
        def _():
            copy_b_hi(j + 1, rows.at[j + 1, t]).wait_recv()
            copy_c(j + 1).start()

        copy_b_lo(j, rows.at[j, t]).wait_recv()
        copy_c(j).wait_recv()

        @pl.loop(0, f_width // f_tile)
        def _(f):
            x = rows[j].reshape(4 * cap, width)
            c = pl.ds(pl.multiple_of(f * f_tile, f_tile), f_tile)
            g = jnp.dot(x, eg[:, c], preferred_element_type=F32)
            u = jnp.dot(x, eu[:, c], preferred_element_type=F32)
            hid[:, c] = (g / (1.0 + jnp.exp(-g)) * u).astype(BF16)

        @pl.loop(0, width // d_tile)
        def _(d):
            c = pl.ds(pl.multiple_of(d * d_tile, d_tile), d_tile)
            y = jnp.dot(hid[...], ed[:, c], preferred_element_type=F32)
            res[j, :, :, c] = y.astype(BF16).reshape(4, cap, d_tile)

        copy_d(j, 0).start()
        copy_d(j, 1).start()

        @pl.when(j >= 1)
        def _():
            step_e(j - 1)

        @pl.when((j >= 1) & (j < n_ep - 1) & (me - j >= 0))
        def _():
            copy_kv(me - j).wait_recv()

            @pl.when(me + 1 < n_ep)
            def _():
                copy_kv(me - j).start()

    step_e(n_ep - 1)

    scale = head_dim ** (-0.5)
    q_tile = span // 2
    run_max[...] = jnp.full_like(run_max, MASKED)
    run_sum[...] = jnp.zeros_like(run_sum)
    run_acc[...] = jnp.zeros_like(run_acc)

    def attend(b, masked):
        kc = pl.ds(pl.multiple_of(b * span, span), span)
        for h in range(heads):
            hc = pl.ds(h * head_dim, head_dim)
            vc = pl.ds(head_width + h * head_dim, head_dim)

            @pl.loop(0, 2)
            def _(i):
                r = pl.ds(pl.multiple_of(i * q_tile, q_tile), q_tile)
                s = lax.dot_general(
                    queries[r, hc], kv[b, :, hc], (((1,), (1,)), ((), ())), preferred_element_type=F32
                )
                s = s * scale + query_gate_ref[r, h : h + 1] - gate_ref[h : h + 1, kc]
                if masked:
                    row = lax.broadcasted_iota(jnp.int32, s.shape, 0) + i * q_tile
                    col = lax.broadcasted_iota(jnp.int32, s.shape, 1)
                    s = jnp.where(col <= row, s, MASKED)
                old = run_max[h, r]
                new = jnp.maximum(old, jnp.max(s, axis=1, keepdims=True))
                w = jnp.exp(s - new)
                fix = jnp.exp(old - new)
                run_max[h, r] = new
                run_sum[h, r] = run_sum[h, r] * fix + jnp.sum(w, axis=1, keepdims=True)
                run_acc[h, r] = run_acc[h, r] * fix + jnp.dot(
                    w.astype(BF16), kv[b, :, vc], preferred_element_type=F32
                )

    attend(me, True)
    if n_ep > 2:

        @pl.loop(0, n_ep - 2)
        def _(j):
            step_f(j)

    @pl.loop(1, me + 1)
    def _(d):
        @pl.when(d == n_ep - 1)
        def _():
            copy_kv(0).wait_recv()

        attend(me - d, False)

    for h in range(heads):
        attended[:, pl.ds(h * head_dim, head_dim)] = (run_acc[h] / run_sum[h]).astype(BF16)
    if n_ep > 1:
        step_f(n_ep - 2)

    loads[3].wait()
    n_relay.wait_send()
    part = seg

    def project(b):
        x = attended[pl.ds(pl.multiple_of(b * mix_rows, mix_rows), mix_rows), :]

        @pl.loop(0, width // d_tile)
        def _(d):
            c = pl.ds(pl.multiple_of(d * d_tile, d_tile), d_tile)
            part[b, :, c] = jnp.dot(x, wo[:, c], preferred_element_type=F32).astype(BF16)

    def copy_m(h):
        return remote(part.at[2 * h + (1 - lo)], mdrec.at[h], ms.at[h], mr.at[h], {"tp": lo_peer})

    m_hi = remote(mdrec.at[other_hi], merec, ms.at[2], mr.at[2], {"tp": hi_peer})
    project(2 * other_hi + (1 - lo))
    copy_m(other_hi).start()
    project(hi_peer)
    project(lo_peer)
    copy_m(hi).start()
    copy_m(other_hi).wait_recv()
    mdrec[other_hi] = (part[hi_peer].astype(F32) + mdrec[other_hi].astype(F32)).astype(BF16)
    m_hi.start()
    project(t)
    step_f(n_ep - 1)
    copy_m(hi).wait_recv()
    m_hi.wait_recv()
    total = part[t].astype(F32) + mdrec[hi].astype(F32) + merec[...].astype(F32)
    inverse = lax.rsqrt(jnp.mean(total * total, axis=-1, keepdims=True) + EPS)
    mixer_ref[...] = (total * inverse * post_gain_ref[...]).astype(BF16)

    n_hi.wait_send()
    n_lo.wait_send()
    copy_m(0).wait_send()
    copy_m(1).wait_send()
    m_hi.wait_send()

    @pl.loop(0, n_ep)
    def _(j):
        @pl.when(j > 0)
        def _():
            copy_a(j).wait_send()
            copy_f(j).wait_send()
            copy_f(j).wait_recv()

        copy_b_hi(j, rows.at[j, t]).wait_send()
        copy_b_lo(j, rows.at[j, t]).wait_send()
        copy_c(j).wait_send()
        copy_d(j, 0).wait_send()
        copy_d(j, 1).wait_send()
        copy_e(j).wait_send()

        @pl.when((j <= me) & (me + 1 < n_ep))
        def _():
            copy_kv(j).wait_send()


def on_device(
    mixer_input,
    forget_cumsum,
    mixer_gain,
    query_weight,
    key_weight,
    value_weight,
    out_weight,
    post_gain,
    expert_input,
    expert_gain,
    routes,
    route_weight,
    expert_gate,
    expert_upward,
    expert_down,
):
    n_ep = lax.axis_size("ep")
    n_tp = lax.axis_size("tp")
    mix_rows, width = mixer_input.shape
    heads = forget_cumsum.shape[0]
    head_width = query_weight.shape[1]
    head_dim = head_width // heads
    span = mix_rows * n_tp
    moe_rows, top_count = routes.shape
    experts_local = expert_gate.shape[0]
    assert n_tp == 4 and experts_local == 1
    experts_all = n_ep
    capacity = (moe_rows * top_count * 9 + 8 * experts_all - 1) // (8 * experts_all)
    cap = (capacity + ROW_TILE - 1) // ROW_TILE * ROW_TILE
    slots_all = experts_all * cap
    first_pos = lax.axis_index("ep") * span

    normed = normalize(mixer_input, mixer_gain).astype(BF16)
    normed_moe = normalize(expert_input, expert_gain).astype(BF16)
    flat_routes = routes.reshape(-1)
    member = (flat_routes[:, None] == jnp.arange(experts_all, dtype=jnp.int32)[None, :]).astype(F32)
    order = jnp.arange(moe_rows * top_count, dtype=jnp.int32)
    earlier = (order[None, :] < order[:, None]).astype(BF16)
    before = jnp.dot(earlier, member.astype(BF16), preferred_element_type=F32)
    slot_rank = jnp.sum(before * member, axis=1).astype(jnp.int32)
    slot_index = (flat_routes * cap + slot_rank).reshape(moe_rows, top_count)
    slot_ids = jnp.arange(slots_all, dtype=jnp.int32)
    choosers = [
        (slot_index[:, which][:, None] == slot_ids[None, :]).astype(BF16) for which in range(top_count)
    ]
    dispatch = functools.reduce(lambda a, b: a + b, choosers)
    outgoing = lax.dot_general(
        dispatch, normed_moe, (((0,), (0,)), ((), ())), preferred_element_type=F32
    ).astype(BF16)
    outgoing = outgoing.reshape(n_ep, cap, width)
    query_gate = lax.dynamic_slice_in_dim(forget_cumsum, first_pos, span, 1).T

    vmem = pl.BlockSpec(memory_space=pltpu.VMEM)
    hbm = pl.BlockSpec(memory_space=pl.ANY)
    dma = pltpu.SemaphoreType.DMA
    f_width = expert_gate.shape[2]
    mixer_output, returned = pl.pallas_call(
        functools.partial(kernel, n_ep, head_dim),
        out_shape=(
            jax.ShapeDtypeStruct((mix_rows, width), BF16),
            jax.ShapeDtypeStruct((n_ep, cap, width), BF16),
        ),
        in_specs=[vmem] * 5 + [hbm] * 7,
        out_specs=(vmem, vmem),
        scratch_shapes=[
            pltpu.VMEM((width, head_width), BF16),
            pltpu.VMEM((width, head_width), BF16),
            pltpu.VMEM((width, head_width), BF16),
            pltpu.VMEM((head_width, width), BF16),
            pltpu.VMEM((width, f_width), BF16),
            pltpu.VMEM((width, f_width), BF16),
            pltpu.VMEM((f_width, width), BF16),
            pltpu.VMEM((4, mix_rows, width), BF16),
            pltpu.VMEM((span, head_width), BF16),
            pltpu.VMEM((n_ep, span, 2 * head_width), BF16),
            pltpu.VMEM((n_ep, 4, cap, width), BF16),
            pltpu.VMEM((4 * cap, f_width), BF16),
            pltpu.VMEM((n_ep, 4, cap, width), BF16),
            pltpu.VMEM((n_ep, 2, cap, width), BF16),
            pltpu.VMEM((n_ep, cap, width), BF16),
            pltpu.VMEM((n_ep, cap, width), BF16),
            pltpu.VMEM((heads, span, 1), F32),
            pltpu.VMEM((heads, span, 1), F32),
            pltpu.VMEM((heads, span, head_dim), F32),
            pltpu.VMEM((span, head_width), BF16),
            pltpu.VMEM((2, mix_rows, width), BF16),
            pltpu.VMEM((mix_rows, width), BF16),
            dma((7,)),
            dma((3,)),
            dma((3,)),
            dma((n_ep,)),
            dma((n_ep,)),
            dma((2, n_ep)),
            dma((2, n_ep)),
            dma((n_ep,)),
            dma((n_ep,)),
            dma((2, n_ep)),
            dma((2, n_ep)),
            dma((n_ep,)),
            dma((n_ep,)),
            dma((n_ep,)),
            dma((n_ep,)),
            dma((n_ep,)),
            dma((n_ep,)),
            dma((3,)),
            dma((3,)),
        ],
        compiler_params=pltpu.CompilerParams(
            collective_id=0, has_side_effects=True, vmem_limit_bytes=66_500_000
        ),
    )(
        normed,
        outgoing,
        query_gate,
        forget_cumsum,
        post_gain.reshape(1, -1),
        query_weight,
        key_weight,
        value_weight,
        out_weight,
        expert_gate[0],
        expert_upward[0],
        expert_down[0],
    )
    returned = returned.reshape(slots_all, width)
    combined = jnp.zeros((moe_rows, width), F32)
    for which in range(top_count):
        picked = jnp.dot(choosers[which], returned, preferred_element_type=F32)
        combined = combined + route_weight[:, which : which + 1] * picked
    return (mixer_output, combined.astype(BF16))


ROW_TILE = 8


def solution(mesh):
    rows = P(("grp", "ep", "tp"), None)
    in_specs = (
        rows,
        P("tp", "grp"),
        P(),
        P(None, "tp"),
        P(None, "tp"),
        P(None, "tp"),
        P("tp", None),
        P(),
        rows,
        P(),
        rows,
        rows,
        P("ep", None, "tp"),
        P("ep", None, "tp"),
        P("ep", "tp", None),
    )
    return jax.shard_map(
        on_device, mesh=mesh, in_specs=in_specs, out_specs=(rows, rows), check_vma=False
    )
```

profile of v0, /device:TPU:9, one launch (start us, length us, event | category | flops | bytes accessed | tf_op | source)
XLA Modules:
  0.0 105.0 jit_solution(12674636994763980484)
XLA Ops:
  0.6 0.0 copy-start.1
  0.6 0.7 constant_dynamic-slice_fusion
  1.4 0.9 copy.29
  2.3 0.8 copy.26
  3.0 0.1 eq.45
  3.2 0.2 fusion.2
  3.4 0.0 copy-start.2
  3.4 0.1 convert_element_type.43
  3.6 0.1 copy.27
  3.6 0.7 multiply_add_fusion
  4.3 1.2 %fusion.6 = f32[128]{0:T(128)S(1)} fusion(bf16[128,2048]{1,0:T(8,128)(2,1)} %param.23), kind=kLoop, calls=%fused_computation.14 | loop fusion | flops 786304 | bytes 524800 | tf_op jit(solution)/shard_map/reduce_sum | solution.py:19
  5.6 0.0 copy-start.4
  5.6 0.0 copy-done.1
  5.6 2.3 %convolution_convert_fusion = bf16[288,2048]{1,0:T(8,128)(2,1)} fusion(bf16[128,2048]{1,0:T(8,128)(2,1)S(1)} %copy-done.1, f32[2048]{0:T(1024)} %param.24, f32[128]{0:T(128)S(1)} %add_rsqrt_fusion, s32[128]{0:T(128)S(1)} %get-tuple-element.9, s32[128]{0:T(128)S(1)} %get-tuple-element.8), kind=kOutput, calls=%fused_computation | convolution fusion | flops 152928256 | bytes 1713664 | tf_op jit(solution)/shard_map/dot_general | solution.py:424
  7.9 0.0 copy-done.2
  7.9 0.2 fusion.3
  8.1 0.0 copy-done.4
  8.1 1.0 fusion.5.normed_ref
  9.1 0.0 copy-start.5
  9.1 92.0 %shard_map.158 = (bf16[128,2048]{1,0:T(8,128)(2,1)}, bf16[4,72,2048]{2,1,0:T(8,128)(2,1)}) custom-call(bf16[128,2048]{1,0:T(8,128)(2,1)} %fusion.5.normed_ref, bf16[4,72,2048]{2,1,0:T(8,128)(2,1)} %bitcast.19, f32[512,2]{1,0:T(8,128)} %bitcast.23, f32[2,2048]{1,0:T(2,128)} %gate_ref.1, f32[1,2048]{1,0:T(1,128)} %bitcast.24, bf16[2048,256]{1,0:T(8,128)(2,1)} %wq_hbm.1, ...), custom_call_target="tpu_custom_call" | custom-call | tf_op jit(solution)/shard_map/pallas_call | solution.py:434
  101.0 0.0 copy-start
  101.0 0.0 copy-done.5
  101.1 1.8 %convolution_multiply_fusion.1 = f32[128,2048]{1,0:T(8,128)S(1)} fusion(bf16[288,2048]{1,0:T(8,128)(2,1)} %bitcast.17, f32[128]{0:T(128)S(1)} %get-tuple-element.7, s32[128]{0:T(128)S(1)} %get-tuple-element.8), kind=kOutput, calls=%fused_computation.3 | convolution fusion | flops 151293952 | bytes 2229248 | tf_op jit(solution)/shard_map/dot_general | solution.py:505
  102.9 0.0 copy-done
  102.9 0.0 copy-start.3
  102.9 1.3 %fusion.1 = bf16[128,2048]{1,0:T(8,128)(2,1)} fusion(f32[128,2048]{1,0:T(8,128)S(1)} %convolution_multiply_fusion.1, bf16[288,2048]{1,0:T(8,128)(2,1)S(1)} %bitcast.18, f32[128]{0:T(128)S(1)} %get-tuple-element.6, s32[128]{0:T(128)S(1)} %get-tuple-element.9), kind=kOutput, calls=%fused_computation.4 | convolution fusion | flops 151818240 | bytes 2753536 | tf_op jit(solution)/shard_map/dot_general | solution.py:505
  104.2 0.0 copy-done.3
  104.2 0.8 copy.31
  (5 shorter events, 0.0 us)
Async XLA Ops:
  0.6 4.9 %copy-start.1 = (bf16[128,2048]{1,0:T(8,128)(2,1)S(1)}, bf16[128,2048]{1,0:T(8,128)(2,1)}, u32[]{:S(2)}) copy-start(bf16[128,2048]{1,0:T(8,128)(2,1)} %param.23) | copy-start | bytes 1572868
  3.4 4.5 %copy-start.2 = (bf16[128,2048]{1,0:T(8,128)(2,1)S(1)}, bf16[128,2048]{1,0:T(8,128)(2,1)}, u32[]{:S(2)}) copy-start(bf16[128,2048]{1,0:T(8,128)(2,1)} %param.15) | copy-start | bytes 1572868
  5.6 2.5 %copy-start.4 = (f32[2048]{0:T(1024)S(1)}, f32[2048]{0:T(1024)}, u32[]{:S(2)}) copy-start(f32[2048]{0:T(1024)} %param.17) | copy-start | bytes 24580
  9.1 92.0 %copy-start.5 = (f32[128,2]{0,1:T(2,128)S(1)}, f32[128,2]{0,1:T(2,128)}, u32[]{:S(2)}) copy-start(f32[128,2]{0,1:T(2,128)} %param.26) | copy-start | bytes 3076
  101.0 1.9 %copy-start = (bf16[4,72,2048]{2,1,0:T(8,128)(2,1)S(1)}, bf16[4,72,2048]{2,1,0:T(8,128)(2,1)}, u32[]{:S(2)}) copy-start(bf16[4,72,2048]{2,1,0:T(8,128)(2,1)} %get-tuple-element.5) | copy-start | bytes 3538948
  102.9 1.3 %copy-start.3 = (bf16[128,2048]{1,0:T(8,128)(2,1)S(1)}, bf16[128,2048]{1,0:T(8,128)(2,1)}, u32[]{:S(2)}) copy-start(bf16[128,2048]{1,0:T(8,128)(2,1)} %get-tuple-element.12) | copy-start | bytes 1572868
where the time goes:
time: 105 us
  Pallas kernels  92 us (88%)
  matrix products  5.62 us (5%)
  local copies, waits for them, and re-layouts  3.56 us (3%)
  other arithmetic  3.12 us (3%)
    pallas_call x1, Pallas kernels, on_device(): pl.pallas_call(functools.partial(kernel, n_ep, head_dim), out_shape=(jax....  92 us
    dot_general x2, matrix products, on_device(): picked = jnp.dot(choosers[which], returned, preferred_element_type=F32)  3.13 us
    unnamed x15, local copies, waits for them, and re-layouts  2.47 us
    dot_general x1, matrix products, on_device(): lax.dot_general(dispatch, normed_moe, (((0,), (0,)), ((), ())), preferred...  2.29 us

commit v1 on v0

v1 whole, which is shorter than its diff:
```python
import functools

import jax
import jax.numpy as jnp
from jax import lax
from jax.experimental import pallas as pl
from jax.experimental.pallas import tpu as pltpu
from jax.sharding import PartitionSpec as P

EPS = 1e-06
MASKED = -1e30
MESH = pl.DeviceIdType.MESH
F32 = jnp.float32
BF16 = jnp.bfloat16
ROW_TILE = 8
LANES = 128
LOG2_E = 1.4426950408889634


def normalize(row_block, gain):
    values = row_block.astype(F32)
    inverse = lax.rsqrt(jnp.mean(values * values, axis=-1, keepdims=True) + EPS)
    return values * inverse * gain


def iota(shape, dim):
    return lax.broadcasted_iota(jnp.int32, shape, dim)


def columns_of(rows):
    spread = jnp.broadcast_to(rows[0:1], (LANES, rows.shape[1]))
    which = iota(spread.shape, 0)
    for h in range(1, rows.shape[0]):
        spread = jnp.where(which == h, rows[h : h + 1], spread)
    return spread.T


def kernel(
    n_ep,
    head_dim,
    refs,
):
    r = refs
    me = lax.axis_index("ep")
    t = lax.axis_index("tp")
    hi = t // 2
    lo = t % 2
    lo_peer = 2 * hi + (1 - lo)
    hi_peer = 2 * (1 - hi) + lo
    other_hi = 1 - hi
    seg, queries, kv, rows, out = r["seg"], r["queries"], r["kv"], r["rows"], r["out"]
    hid, res, drec, erec, fin, ret = r["hid"], r["res"], r["drec"], r["erec"], out, r["ret"]
    run_max, run_sum, run_acc, attended = r["run_max"], r["run_sum"], r["run_acc"], r["attended"]
    mdrec, merec, gate, columns = r["mdrec"], r["mixer_input"], r["gate"], r["columns"]
    wq, wk, wv, wo, eg, eu, ed = (r[k] for k in ("wq", "wk", "wv", "wo", "eg", "eu", "ed"))
    mix_rows, width = r["mixer_out"].shape
    head_width = wq.shape[1]
    heads = head_width // head_dim
    span = 4 * mix_rows
    cap = out.shape[1]
    top_count, moe_rows = r["routes"].shape
    folded = n_ep == 4

    def remote(src, dst, send_sem, recv_sem, where):
        return pltpu.make_async_remote_copy(
            src_ref=src,
            dst_ref=dst,
            send_sem=send_sem,
            recv_sem=recv_sem,
            device_id=where,
            device_id_type=MESH,
        )

    names = (
        "mixer_input", "mixer_gain", "routes", "expert_input", "expert_gain", "wq", "wk", "wv",
        "eg", "eu", "ed", "route_weight", "gate", "post_gain", "wo",
    )
    loads = {
        name: pltpu.make_async_copy(r[name + "_hbm"], r[name], r["load_sem"].at[i])
        for i, name in enumerate(names)
    }
    barrier = pltpu.get_barrier_semaphore()
    pl.semaphore_signal(barrier, inc=1, device_id={"tp": lo_peer}, device_id_type=MESH)
    pl.semaphore_signal(barrier, inc=1, device_id={"tp": hi_peer}, device_id_type=MESH)

    @pl.loop(1, n_ep)
    def _(j):
        pl.semaphore_signal(barrier, inc=1, device_id={"ep": lax.rem(me + j, n_ep)}, device_id_type=MESH)

    for name in names:
        loads[name].start()

    n_hi = remote(seg.at[t], seg.at[t], r["ns"].at[0], r["nr"].at[0], {"tp": hi_peer})
    n_lo = remote(seg.at[t], seg.at[t], r["ns"].at[1], r["nr"].at[1], {"tp": lo_peer})
    n_relay = remote(seg.at[hi_peer], seg.at[hi_peer], r["ns"].at[2], r["nr"].at[2], {"tp": lo_peer})
    diag_peer = 2 * other_hi + (1 - lo)

    def copy_a(to):
        return remote(out.at[to], rows.at[me, t], r["as"].at[to], r["ar"].at[me], {"ep": to})

    def recv_a(s):
        return remote(out.at[s], rows.at[s, t], r["as"].at[s], r["ar"].at[s], {"ep": s})

    def copy_b_hi(s):
        return remote(rows.at[s, t], rows.at[s, t], r["bs"].at[0, s], r["br"].at[0, s], {"tp": hi_peer})

    def copy_b_lo(s):
        return remote(rows.at[s, t], rows.at[s, t], r["bs"].at[1, s], r["br"].at[1, s], {"tp": lo_peer})

    def copy_c(s):
        return remote(rows.at[s, hi_peer], rows.at[s, hi_peer], r["cs"].at[s], r["cr"].at[s], {"tp": lo_peer})

    def copy_d(s, h):
        return remote(res.at[s, 2 * h + (1 - lo)], drec.at[s, h], r["ds"].at[h, s], r["dr"].at[h, s], {"tp": lo_peer})

    def copy_e(s):
        return remote(drec.at[s, other_hi], erec.at[s], r["es"].at[s], r["er"].at[s], {"tp": hi_peer})

    def copy_f(s):
        return remote(fin.at[s], ret.at[me], r["fs"].at[s], r["fr"].at[me], {"ep": s})

    def recv_f(e):
        return remote(fin.at[e], ret.at[e], r["fs"].at[e], r["fr"].at[e], {"ep": e})

    def copy_kv(b, to):
        return remote(kv.at[b], kv.at[b], r["ks"].at[b], r["kr"].at[b], {"ep": to})

    loads["mixer_input"].wait()
    loads["mixer_gain"].wait()
    seg[t] = normalize(r["mixer_input"][...], r["mixer_gain"][...]).astype(BF16)
    pl.semaphore_wait(barrier, 2 + n_ep - 1)
    n_hi.start()
    n_lo.start()

    loads["routes"].wait()
    loads["expert_input"].wait()
    loads["expert_gain"].wait()
    experts = (n_ep + 15) // 16 * 16
    expert_ids = iota((experts, moe_rows), 0)
    chosen = [expert_ids == r["routes"][k : k + 1, :] for k in range(top_count)]
    member = functools.reduce(jnp.logical_or, chosen)
    earlier = jnp.where(iota((moe_rows, moe_rows), 0) < iota((moe_rows, moe_rows), 1), 1.0, 0.0)
    rank = jnp.dot(
        jnp.where(member, 1.0, 0.0).astype(BF16), earlier.astype(BF16), preferred_element_type=F32
    )
    slot = jnp.where(member, rank, -1.0)
    slot_rows = iota((cap, moe_rows), 0).astype(F32)
    for e in range(n_ep):
        r["dispatch"][e] = jnp.where(slot[e : e + 1, :] == slot_rows, 1.0, 0.0).astype(BF16)
    normed_moe = r["expert_input"]
    normed_moe[...] = normalize(normed_moe[...], r["expert_gain"][...]).astype(BF16)

    sent = r["dispatch"][...].reshape(n_ep * cap, moe_rows)
    out[...] = jnp.dot(sent, normed_moe[...], preferred_element_type=F32).astype(BF16).reshape(out.shape)
    if folded:
        s1 = me + 1 - 2 * (me % 2)
        s2 = jnp.where(me < 2, 3, 0)
        s3 = jnp.where(me < 2, 2, 1)
        for s in (s1, s2, s3):
            copy_a(s).start()
    else:

        @pl.loop(1, n_ep)
        def _(j):
            copy_a(lax.rem(me + j, n_ep)).start()

    rows[me, t] = out[me]
    copy_b_hi(me).start()
    copy_b_lo(me).start()

    loads["route_weight"].wait()
    weight = functools.reduce(
        lambda a, b: a + b,
        [jnp.where(chosen[k], r["route_weight"][k : k + 1, :], 0.0) for k in range(top_count)],
    )

    def turned(x):
        return jnp.concatenate([x, jnp.zeros((LANES - experts, moe_rows), F32)], axis=0).T

    slot_turned = turned(slot)
    r["weights"][...] = turned(weight)
    slot_columns = iota((moe_rows, cap), 1).astype(F32)
    for e in range(n_ep):
        r["pick"][e] = jnp.where(slot_turned[:, e : e + 1] == slot_columns, 1.0, 0.0).astype(BF16)

    def combine(e, first):
        weights = r["weights"][...]
        share = jnp.sum(jnp.where(iota(weights.shape, 1) == e, weights, 0.0), axis=1, keepdims=True)

        y = share * jnp.dot(r["pick"][e], ret[e], preferred_element_type=F32)
        r["combined"][...] = y if first else r["combined"][...] + y

    def project_in(half):
        x = seg[pl.ds(2 * half, 2)].reshape(2 * mix_rows, width)
        p = pl.ds(pl.multiple_of(half * 2 * mix_rows, 2 * mix_rows), 2 * mix_rows)
        kv[me, p, pl.ds(0, head_width)] = jnp.dot(x, wk[...], preferred_element_type=F32).astype(BF16)
        kv[me, p, pl.ds(head_width, head_width)] = jnp.dot(x, wv[...], preferred_element_type=F32).astype(BF16)
        queries[p, :] = jnp.dot(x, wq[...], preferred_element_type=F32).astype(BF16)

    def expert(s, half):
        x = rows[s, pl.ds(2 * half, 2)].reshape(2 * cap, width)
        g = jnp.dot(x, eg[...], preferred_element_type=F32)
        u = jnp.dot(x, eu[...], preferred_element_type=F32)
        hid[...] = (g / (1.0 + jnp.exp(-g)) * u).astype(BF16)
        y = jnp.dot(hid[...], ed[...], preferred_element_type=F32)
        res[s, pl.ds(2 * half, 2)] = y.astype(BF16).reshape(2, cap, width)
        copy_d(s, half).start()

    def step_e(s):
        copy_d(s, other_hi).wait_recv()
        drec[s, other_hi] = (res[s, hi_peer].astype(F32) + drec[s, other_hi].astype(F32)).astype(BF16)
        copy_e(s).start()

    def step_f(s, own):
        copy_d(s, hi).wait_recv()
        copy_e(s).wait_recv()
        total = (res[s, t].astype(F32) + drec[s, hi].astype(F32) + erec[s].astype(F32)).astype(BF16)
        if own:
            ret[s] = total
        else:
            copy_a(s).wait_send()
            fin[s] = total
            copy_f(s).start()

    scale = head_dim ** (-0.5) * LOG2_E

    def block(b):
        return pl.ds(pl.multiple_of(b * span, span), span)

    def attend(q, qb, b, cols, i, masked, first):
        for h in range(heads):
            hc = pl.ds(h * head_dim, head_dim)
            vc = pl.ds(head_width + h * head_dim, head_dim)
            s = lax.dot_general(kv[b, :, hc], q[:, hc], (((1,), (1,)), ((), ())), preferred_element_type=F32)
            s = s * scale + (gate[h : h + 1, block(qb)] - cols[:, h : h + 1])
            if masked:
                s = jnp.where(iota(s.shape, 0) <= iota(s.shape, 1), s, MASKED)
            new = jnp.max(s, axis=0, keepdims=True)
            if not first:
                old = run_max[i, h : h + 1]
                new = jnp.maximum(old, new)
                fix = jnp.exp2(old - new)
            w = jnp.exp2(s - new)
            part_sum = jnp.sum(w, axis=0, keepdims=True)
            part_acc = lax.dot_general(
                kv[b, :, vc], w.astype(BF16), (((0,), (0,)), ((), ())), preferred_element_type=F32
            )
            run_max[i, h : h + 1] = new
            if first:
                run_sum[i, h : h + 1] = part_sum
                run_acc[i, h] = part_acc
            else:
                run_sum[i, h : h + 1] = run_sum[i, h : h + 1] * fix + part_sum
                run_acc[i, h] = run_acc[i, h] * fix + part_acc

    def finish():
        for h in range(heads):
            mean = run_acc[0, h] / run_sum[0, h : h + 1]
            attended[:, pl.ds(h * head_dim, head_dim)] = mean.T.astype(BF16)

    def load_gate():
        loads["gate"].wait()
        gate[...] = gate[...] * LOG2_E

    def gate_columns(i, b):
        columns[i] = columns_of(gate[:, block(b)])

    part = seg

    def project(b):
        x = attended[pl.ds(pl.multiple_of(b * mix_rows, mix_rows), mix_rows), :]

        part[b] = jnp.dot(x, wo[...], preferred_element_type=F32).astype(BF16)

    def copy_m(h):
        return remote(part.at[2 * h + (1 - lo)], mdrec.at[h], r["ms"].at[h], r["mr"].at[h], {"tp": lo_peer})

    m_hi = remote(mdrec.at[other_hi], merec, r["ms"].at[2], r["mr"].at[2], {"tp": hi_peer})

    def mix_out():
        loads["wo"].wait()
        n_hi.wait_send()
        n_lo.wait_send()
        n_relay.wait_send()
        project(diag_peer)
        copy_m(other_hi).start()
        project(hi_peer)
        copy_m(other_hi).wait_recv()
        mdrec[other_hi] = (part[hi_peer].astype(F32) + mdrec[other_hi].astype(F32)).astype(BF16)
        m_hi.start()
        project(lo_peer)
        copy_m(hi).start()
        project(t)

    def mix_end():
        copy_m(hi).wait_recv()
        loads["post_gain"].wait()
        m_hi.wait_recv()
        total = part[t].astype(F32) + mdrec[hi].astype(F32) + merec[...].astype(F32)
        inverse = lax.rsqrt(jnp.mean(total * total, axis=-1, keepdims=True) + EPS)
        r["mixer_out"][...] = (total * inverse * r["post_gain"][...]).astype(BF16)

    def relay_b(s):
        recv_a(s).wait_recv()
        copy_b_hi(s).start()
        copy_b_lo(s).start()

    def relay_c(s):
        copy_b_hi(s).wait_recv()
        copy_c(s).start()

    def expert_own(s):
        copy_b_lo(s).wait_recv()
        expert(s, hi)

    def expert_other(s):
        copy_c(s).wait_recv()
        expert(s, other_hi)

    if folded:
        qin, obuf, lbuf, oin, lin = r["qin"], r["obuf"], r["lbuf"], r["oin"], r["lin"]
        helper = me == 1
        odd = me % 2 == 1
        asks = me >= 2

        def copy_q():
            return remote(queries, qin.at[me - 2], r["qs"].at[0], r["qr"].at[me - 2], {"ep": 1})

        def recv_q(i):
            return remote(queries, qin.at[i], r["qs"].at[0], r["qr"].at[i], {"ep": 1})

        def copy_o(i):
            return remote(obuf.at[i], oin, r["os"].at[0, i], r["or"].at[0], {"ep": 2 + i})

        def copy_l(i):
            return remote(lbuf.at[i], lin, r["os"].at[1, i], r["or"].at[1], {"ep": 2 + i})

        for name in ("wq", "wk", "wv"):
            loads[name].wait()
        n_lo.wait_recv()
        project_in(hi)
        for name in ("eg", "eu", "ed"):
            loads[name].wait()
        expert_own(me)
        load_gate()
        gate_columns(0, me)

        @pl.when(odd)
        def _():
            gate_columns(1, me - 1)

        relay_b(s1)
        n_hi.wait_recv()
        n_relay.start()
        expert_own(s1)
        n_relay.wait_recv()
        project_in(other_hi)

        @pl.when(asks)
        def _():
            copy_q().start()

        @pl.when(me % 2 == 0)
        def _():
            copy_kv(me, me + 1).start()

        relay_c(me)
        attend(queries, me, me, columns.at[0], 0, True, True)
        relay_b(s2)
        expert_other(me)
        expert_own(s2)
        relay_c(s1)
        expert_other(s1)
        step_e(s1)

        @pl.when(helper)
        def _():
            for i in range(2):
                recv_q(i).wait_recv()
                attend(qin.at[i], 2 + i, me, columns.at[0], 1 + i, False, True)

        relay_c(s2)
        expert_other(s2)
        step_e(s2)
        relay_b(s3)

        @pl.when(odd)
        def _():
            copy_kv(me - 1, me).wait_recv()

        @pl.when(helper)
        def _():
            for i in range(2):
                attend(qin.at[i], 2 + i, 0, columns.at[1], 1 + i, False, False)
                for h in range(heads):
                    total = run_sum[1 + i, h : h + 1]
                    obuf[i, pl.ds(h * head_dim, head_dim)] = (run_acc[1 + i, h] / total).astype(BF16)
                    lbuf[i, h : h + 1] = run_max[1 + i, h : h + 1] + jnp.log2(total)
                copy_o(i).start()
                copy_l(i).start()

        @pl.when(odd)
        def _():
            attend(queries, me, me - 1, columns.at[1], 0, False, False)

        expert_own(s3)

        @pl.when(me < 2)
        def _():
            finish()

        step_f(s1, False)
        relay_c(s3)
        expert_other(s3)
        step_e(s3)
        step_e(me)
        step_f(s2, False)

        @pl.when(asks)
        def _():
            copy_o(me - 2).wait_recv()
            copy_l(me - 2).wait_recv()
            for h in range(heads):
                hc = pl.ds(h * head_dim, head_dim)
                far, old = lin[h : h + 1], run_max[0, h : h + 1]
                new = jnp.maximum(old, far)
                fix, far_fix = jnp.exp2(old - new), jnp.exp2(far - new)
                numer = run_acc[0, h] * fix + oin[hc].astype(F32) * far_fix
                attended[:, hc] = (numer / (run_sum[0, h : h + 1] * fix + far_fix)).T.astype(BF16)

        mix_out()
        step_f(s3, False)
        step_f(me, True)
        combine(me, True)
        for e in (s1, s2, s3):
            recv_f(e).wait_recv()
            combine(e, False)
        r["expert_out"][...] = r["combined"][...].astype(BF16)
        mix_end()

        @pl.when(asks)
        def _():
            copy_q().wait_send()

        @pl.when(me % 2 == 0)
        def _():
            copy_kv(me, me + 1).wait_send()

        @pl.when(helper)
        def _():
            for i in range(2):
                copy_o(i).wait_send()
                copy_l(i).wait_send()

    else:
        step = lambda j: lax.rem(me + j, n_ep)
        for name in ("wq", "wk", "wv"):
            loads[name].wait()
        n_hi.wait_recv()
        n_relay.start()
        n_lo.wait_recv()
        project_in(hi)
        n_relay.wait_recv()
        project_in(other_hi)

        @pl.when(me + 1 < n_ep)
        def _():
            copy_kv(me, me + 1).start()

        for name in ("eg", "eu", "ed"):
            loads[name].wait()
        load_gate()
        gate_columns(0, me)

        @pl.loop(0, n_ep)
        def _(j):
            s = step(j)

            @pl.when(j + 1 < n_ep)
            def _():
                relay_b(step(j + 1))

            expert_own(s)
            relay_c(s)
            expert_other(s)

            @pl.when(j >= 1)
            def _():
                step_e(step(j - 1))

            @pl.when((j >= 1) & (j < n_ep - 1) & (me - j >= 0))
            def _():
                copy_kv(me - j, me).wait_recv()

                @pl.when(me + 1 < n_ep)
                def _():
                    copy_kv(me - j, me + 1).start()

        step_e(step(n_ep - 1))
        attend(queries, me, me, columns.at[0], 0, True, True)
        step_f(me, True)
        combine(me, True)

        @pl.loop(1, n_ep)
        def _(j):
            step_f(step(j), False)

        @pl.loop(1, me + 1)
        def _(d):
            @pl.when(d == n_ep - 1)
            def _():
                copy_kv(0, me).wait_recv()

            gate_columns(0, me - d)
            attend(queries, me, me - d, columns.at[0], 0, False, False)

        finish()
        mix_out()

        @pl.loop(1, n_ep)
        def _(j):
            recv_f(step(j)).wait_recv()
            combine(step(j), False)

        r["expert_out"][...] = r["combined"][...].astype(BF16)
        mix_end()

        @pl.when(me + 1 < n_ep)
        def _():
            @pl.loop(0, me + 1)
            def _(b):
                copy_kv(b, me + 1).wait_send()

    copy_m(0).wait_send()
    copy_m(1).wait_send()
    m_hi.wait_send()

    @pl.loop(0, n_ep)
    def _(j):
        s = lax.rem(me + j, n_ep)

        @pl.when(j > 0)
        def _():
            copy_f(s).wait_send()

        copy_b_hi(s).wait_send()
        copy_b_lo(s).wait_send()
        copy_c(s).wait_send()
        copy_d(s, 0).wait_send()
        copy_d(s, 1).wait_send()
        copy_e(s).wait_send()


def on_device(
    mixer_input,
    forget_cumsum,
    mixer_gain,
    query_weight,
    key_weight,
    value_weight,
    out_weight,
    post_gain,
    expert_input,
    expert_gain,
    routes,
    route_weight,
    expert_gate,
    expert_upward,
    expert_down,
):
    n_ep = lax.axis_size("ep")
    n_tp = lax.axis_size("tp")
    mix_rows, width = mixer_input.shape
    heads = forget_cumsum.shape[0]
    head_width = query_weight.shape[1]
    head_dim = head_width // heads
    span = mix_rows * n_tp
    moe_rows, top_count = routes.shape
    assert n_tp == 4 and expert_gate.shape[0] == 1
    capacity = (moe_rows * top_count * 9 + 8 * n_ep - 1) // (8 * n_ep)
    cap = (capacity + ROW_TILE - 1) // ROW_TILE * ROW_TILE
    f_width = expert_gate.shape[2]
    folded = n_ep == 4
    sets = 3 if folded else 1

    inputs = {
        "mixer_input": mixer_input,
        "mixer_gain": mixer_gain.reshape(1, -1),
        "routes": routes.T,
        "expert_input": expert_input,
        "expert_gain": expert_gain.reshape(1, -1),
        "wq": query_weight,
        "wk": key_weight,
        "wv": value_weight,
        "eg": expert_gate[0],
        "eu": expert_upward[0],
        "ed": expert_down[0],
        "route_weight": route_weight.T,
        "gate": forget_cumsum,
        "post_gain": post_gain.reshape(1, -1),
        "wo": out_weight,
    }
    vmem, dma = pltpu.VMEM, pltpu.SemaphoreType.DMA
    scratch = {name: vmem(x.shape, x.dtype) for name, x in inputs.items()}
    scratch |= {
        "seg": vmem((4, mix_rows, width), BF16),
        "queries": vmem((span, head_width), BF16),
        "kv": vmem((n_ep, span, 2 * head_width), BF16),
        "rows": vmem((n_ep, 4, cap, width), BF16),
        "out": vmem((n_ep, cap, width), BF16),
        "dispatch": vmem((n_ep, cap, moe_rows), BF16),
        "pick": vmem((n_ep, moe_rows, cap), BF16),
        "weights": vmem((moe_rows, LANES), F32),
        "combined": vmem((moe_rows, width), F32),
        "hid": vmem((2 * cap, f_width), BF16),
        "res": vmem((n_ep, 4, cap, width), BF16),
        "drec": vmem((n_ep, 2, cap, width), BF16),
        "erec": vmem((n_ep, cap, width), BF16),
        "ret": vmem((n_ep, cap, width), BF16),
        "run_max": vmem((sets, heads, span), F32),
        "run_sum": vmem((sets, heads, span), F32),
        "run_acc": vmem((sets, heads, head_dim, span), F32),
        "attended": vmem((span, head_width), BF16),
        "columns": vmem((2 if folded else 1, span, LANES), F32),
        "mdrec": vmem((2, mix_rows, width), BF16),
        "load_sem": dma((len(inputs),)),
    }
    if folded:
        scratch |= {
            "qin": vmem((2, span, head_width), BF16),
            "obuf": vmem((2, head_width, span), BF16),
            "lbuf": vmem((2, 8, span), F32),
            "oin": vmem((head_width, span), BF16),
            "lin": vmem((8, span), F32),
            "qs": dma((1,)),
            "qr": dma((2,)),
            "os": dma((2, 2)),
            "or": dma((2,)),
        }
    scratch |= {"ns": dma((3,)), "nr": dma((3,)), "ms": dma((3,)), "mr": dma((3,))}
    for name in ("a", "c", "e", "f", "k"):
        scratch |= {name + "s": dma((n_ep,)), name + "r": dma((n_ep,))}
    for name in ("b", "d"):
        scratch |= {name + "s": dma((2, n_ep)), name + "r": dma((2, n_ep))}

    labels = [name + "_hbm" for name in inputs] + ["mixer_out", "expert_out"] + list(scratch)

    def body(*refs):
        kernel(n_ep, head_dim, dict(zip(labels, refs, strict=True)))

    block = pl.BlockSpec(memory_space=pltpu.VMEM)
    return pl.pallas_call(
        body,
        out_shape=(
            jax.ShapeDtypeStruct((mix_rows, width), BF16),
            jax.ShapeDtypeStruct((moe_rows, width), BF16),
        ),
        in_specs=[pl.BlockSpec(memory_space=pl.ANY)] * len(inputs),
        out_specs=(block, block),
        scratch_shapes=list(scratch.values()),
        compiler_params=pltpu.CompilerParams(
            collective_id=0, has_side_effects=True, vmem_limit_bytes=66_500_000
        ),
    )(*inputs.values())


def solution(mesh):
    rows = P(("grp", "ep", "tp"), None)
    in_specs = (
        rows,
        P("tp", "grp"),
        P(),
        P(None, "tp"),
        P(None, "tp"),
        P(None, "tp"),
        P("tp", None),
        P(),
        rows,
        P(),
        rows,
        rows,
        P("ep", None, "tp"),
        P("ep", None, "tp"),
        P("ep", "tp", None),
    )
    return jax.shard_map(
        on_device, mesh=mesh, in_specs=in_specs, out_specs=(rows, rows), check_vma=False
    )
```

time: 105 us -> 96.6 us (0.920)
  the two profiles are of different devices: /device:TPU:9 before, /device:TPU:0 now
where the time goes in v1:
time: 96.6 us; the launch traced here: 94.7 us
  Pallas kernels  90.3 us (93%)
  local copies, waits for them, and re-layouts  3.76 us (4%)
    pallas_call x1, Pallas kernels, on_device(): pl.pallas_call(body, out_shape=(jax.ShapeDtypeStruct((mix_rows, width), B...  90.3 us
    unnamed x2, local copies, waits for them, and re-layouts  3.76 us

profile of v1, /device:TPU:0, one launch (start us, length us, event | category | flops | bytes accessed | tf_op | source)
XLA Modules:
  0.0 94.7 jit_solution(16007787425087146569)
XLA Ops:
  0.6 90.3 %shard_map.158 = (bf16[128,2048]{1,0:T(8,128)(2,1)}, bf16[128,2048]{1,0:T(8,128)(2,1)}) custom-call(bf16[128,2048]{1,0:T(8,128)(2,1)} %refs_0_.1, f32[1,2048]{1,0:T(1,128)} %bitcast.11, s32[2,128]{1,0:T(2,128)} %bitcast.14, bf16[128,2048]{1,0:T(8,128)(2,1)} %refs_3_.1, f32[1,2048]{1,0:T(1,128)} %bitcast.12, bf16[2048,256]{1,0:T(8,128)(2,1)} %refs_5_.1, ...), custom_call_target="tpu_custom_call" | custom-call | tf_op jit(solution)/shard_map/pallas_call | solution.py:652
  90.9 1.9 %copy.19 = bf16[128,2048]{1,0:T(8,128)(2,1)} copy(bf16[128,2048]{1,0:T(8,128)(2,1)} %get-tuple-element.4) | data formatting | bytes 1048576
  92.8 1.9 %copy.20 = bf16[128,2048]{1,0:T(8,128)(2,1)} copy(bf16[128,2048]{1,0:T(8,128)(2,1)} %get-tuple-element.5) | data formatting | bytes 1048576

commit v2 on v1

--- a/solution.py
+++ b/solution.py
@@ -153,11 +153,17 @@
     sent = r["dispatch"][...].reshape(n_ep * cap, moe_rows)
     out[...] = jnp.dot(sent, normed_moe[...], preferred_element_type=F32).astype(BF16).reshape(out.shape)
     if folded:
-        s1 = me + 1 - 2 * (me % 2)
-        s2 = jnp.where(me < 2, 3, 0)
-        s3 = jnp.where(me < 2, 2, 1)
-        for s in (s1, s2, s3):
-            copy_a(s).start()
+        inner = (me > 0) & (me < n_ep - 1)
+        edge = jnp.logical_not(inner)
+        p1 = 1 + me % 2
+        p2 = jnp.where(me < 2, 2 - 2 * me, 3 - 2 * (me - 2))
+        p3 = jnp.where(me < 2, 3, 0)
+        copy_a(p1).start()
+
+        @pl.when(inner)
+        def _():
+            copy_a(p2).start()
+
     else:
 
         @pl.loop(1, n_ep)
@@ -319,21 +325,10 @@
 
     if folded:
         qin, obuf, lbuf, oin, lin = r["qin"], r["obuf"], r["lbuf"], r["oin"], r["lin"]
-        helper = me == 1
-        odd = me % 2 == 1
-        asks = me >= 2
-
-        def copy_q():
-            return remote(queries, qin.at[me - 2], r["qs"].at[0], r["qr"].at[me - 2], {"ep": 1})
-
-        def recv_q(i):
-            return remote(queries, qin.at[i], r["qs"].at[0], r["qr"].at[i], {"ep": 1})
-
-        def copy_o(i):
-            return remote(obuf.at[i], oin, r["os"].at[0, i], r["or"].at[0], {"ep": 2 + i})
-
-        def copy_l(i):
-            return remote(lbuf.at[i], lin, r["os"].at[1, i], r["or"].at[1], {"ep": 2 + i})
+        first, second, helper, last = me == 0, me == 1, me == 2, me == 3
+        copy_q = remote(queries, qin, r["qs"].at[0], r["qr"].at[0], {"ep": 2})
+        copy_o = remote(obuf, oin, r["os"].at[0], r["or"].at[0], {"ep": 3})
+        copy_l = remote(lbuf, lin, r["os"].at[1], r["or"].at[1], {"ep": 3})
 
         for name in ("wq", "wk", "wv"):
             loads[name].wait()
@@ -345,81 +340,124 @@
         load_gate()
         gate_columns(0, me)
 
-        @pl.when(odd)
+        @pl.when(inner)
         def _():
             gate_columns(1, me - 1)
 
-        relay_b(s1)
+        @pl.when(helper)
+        def _():
+            gate_columns(2, 0)
+
+        relay_b(p1)
+
+        @pl.when(inner)
+        def _():
+            relay_b(p2)
+
+        @pl.when(edge)
+        def _():
+            copy_a(p2).start()
+
+        copy_a(p3).start()
         n_hi.wait_recv()
         n_relay.start()
-        expert_own(s1)
+        expert_own(p1)
         n_relay.wait_recv()
         project_in(other_hi)
 
-        @pl.when(asks)
-        def _():
-            copy_q().start()
-
-        @pl.when(me % 2 == 0)
-        def _():
-            copy_kv(me, me + 1).start()
-
+        @pl.when(first)
+        def _():
+            copy_kv(0, 1).start()
+
+        @pl.when(last)
+        def _():
+            copy_q.start()
+
+        attend(queries, me, me, columns.at[0], 0, True, True)
         relay_c(me)
-        attend(queries, me, me, columns.at[0], 0, True, True)
-        relay_b(s2)
         expert_other(me)
-        expert_own(s2)
-        relay_c(s1)
-        expert_other(s1)
-        step_e(s1)
+
+        @pl.when(second)
+        def _():
+            copy_kv(1, 2).start()
+
+        @pl.when(inner)
+        def _():
+            expert_own(p2)
+
+        @pl.when(edge)
+        def _():
+            step_e(me)
+
+        relay_c(p1)
+        expert_other(p1)
+        step_e(p1)
+
+        @pl.when(edge)
+        def _():
+            relay_b(p2)
+
+        relay_b(p3)
+
+        @pl.when(edge)
+        def _():
+            expert_own(p2)
 
         @pl.when(helper)
         def _():
-            for i in range(2):
-                recv_q(i).wait_recv()
-                attend(qin.at[i], 2 + i, me, columns.at[0], 1 + i, False, True)
-
-        relay_c(s2)
-        expert_other(s2)
-        step_e(s2)
-        relay_b(s3)
-
-        @pl.when(odd)
-        def _():
-            copy_kv(me - 1, me).wait_recv()
+            copy_q.wait_recv()
+            attend(qin, 3, 2, columns.at[0], 1, False, True)
+
+        expert_own(p3)
+
+        @pl.when(second)
+        def _():
+            copy_kv(0, 1).wait_recv()
+            copy_kv(0, 2).start()
+            attend(queries, 1, 0, columns.at[1], 0, False, False)
+
+        relay_c(p2)
+        expert_other(p2)
+        step_e(p2)
 
         @pl.when(helper)
         def _():
-            for i in range(2):
-                attend(qin.at[i], 2 + i, 0, columns.at[1], 1 + i, False, False)
-                for h in range(heads):
-                    total = run_sum[1 + i, h : h + 1]
-                    obuf[i, pl.ds(h * head_dim, head_dim)] = (run_acc[1 + i, h] / total).astype(BF16)
-                    lbuf[i, h : h + 1] = run_max[1 + i, h : h + 1] + jnp.log2(total)
-                copy_o(i).start()
-                copy_l(i).start()
-
-        @pl.when(odd)
-        def _():
-            attend(queries, me, me - 1, columns.at[1], 0, False, False)
-
-        expert_own(s3)
-
-        @pl.when(me < 2)
+            copy_kv(1, 2).wait_recv()
+            attend(queries, 2, 1, columns.at[1], 0, False, False)
+            attend(qin, 3, 1, columns.at[1], 1, False, False)
+
+        relay_c(p3)
+        expert_other(p3)
+        step_e(p3)
+
+        @pl.when(inner)
+        def _():
+            step_e(me)
+
+        step_f(p1, False)
+
+        @pl.when(helper)
+        def _():
+            copy_kv(0, 2).wait_recv()
+            attend(qin, 3, 0, columns.at[2], 1, False, False)
+            for h in range(heads):
+                total = run_sum[1, h : h + 1]
+                obuf[pl.ds(h * head_dim, head_dim)] = (run_acc[1, h] / total).astype(BF16)
+                lbuf[h : h + 1] = run_max[1, h : h + 1] + jnp.log2(total)
+            copy_o.start()
+            copy_l.start()
+            attend(queries, 2, 0, columns.at[2], 0, False, False)
+
+        step_f(p2, False)
+
+        @pl.when(jnp.logical_not(last))
         def _():
             finish()
 
-        step_f(s1, False)
-        relay_c(s3)
-        expert_other(s3)
-        step_e(s3)
-        step_e(me)
-        step_f(s2, False)
-
-        @pl.when(asks)
-        def _():
-            copy_o(me - 2).wait_recv()
-            copy_l(me - 2).wait_recv()
+        @pl.when(last)
+        def _():
+            copy_o.wait_recv()
+            copy_l.wait_recv()
             for h in range(heads):
                 hc = pl.ds(h * head_dim, head_dim)
                 far, old = lin[h : h + 1], run_max[0, h : h + 1]
@@ -429,28 +467,32 @@
                 attended[:, hc] = (numer / (run_sum[0, h : h + 1] * fix + far_fix)).T.astype(BF16)
 
         mix_out()
-        step_f(s3, False)
+        step_f(p3, False)
         step_f(me, True)
         combine(me, True)
-        for e in (s1, s2, s3):
+        for e in (p1, p2, p3):
             recv_f(e).wait_recv()
             combine(e, False)
         r["expert_out"][...] = r["combined"][...].astype(BF16)
         mix_end()
 
-        @pl.when(asks)
-        def _():
-            copy_q().wait_send()
-
-        @pl.when(me % 2 == 0)
-        def _():
-            copy_kv(me, me + 1).wait_send()
+        @pl.when(first)
+        def _():
+            copy_kv(0, 1).wait_send()
+
+        @pl.when(second)
+        def _():
+            copy_kv(1, 2).wait_send()
+            copy_kv(0, 2).wait_send()
 
         @pl.when(helper)
         def _():
-            for i in range(2):
-                copy_o(i).wait_send()
-                copy_l(i).wait_send()
+            copy_o.wait_send()
+            copy_l.wait_send()
+
+        @pl.when(last)
+        def _():
+            copy_q.wait_send()
 
     else:
         step = lambda j: lax.rem(me + j, n_ep)
@@ -549,6 +591,24 @@
         copy_d(s, 0).wait_send()
         copy_d(s, 1).wait_send()
         copy_e(s).wait_send()
+
+
+def hand_out(*refs):
+    sources, places, held, sems = refs[:2], refs[2:4], refs[4:6], refs[6]
+    half = held[0].shape[0] // 2
+    loads, stores = [], []
+    for i, (source, place, part) in enumerate(zip(sources, places, held)):
+        for k in range(2):
+            p = pl.ds(k * half, half)
+            loads.append(pltpu.make_async_copy(source.at[p], part.at[p], sems.at[0, 2 * i + k]))
+            stores.append(pltpu.make_async_copy(part.at[p], place.at[p], sems.at[1, 2 * i + k]))
+    for load in loads:
+        load.start()
+    for load, store in zip(loads, stores):
+        load.wait()
+        store.start()
+    for store in stores:
+        store.wait()
 
 
 def on_device(
@@ -581,7 +641,7 @@
     cap = (capacity + ROW_TILE - 1) // ROW_TILE * ROW_TILE
     f_width = expert_gate.shape[2]
     folded = n_ep == 4
-    sets = 3 if folded else 1
+    sets = 2 if folded else 1
 
     inputs = {
         "mixer_input": mixer_input,
@@ -621,20 +681,20 @@
         "run_sum": vmem((sets, heads, span), F32),
         "run_acc": vmem((sets, heads, head_dim, span), F32),
         "attended": vmem((span, head_width), BF16),
-        "columns": vmem((2 if folded else 1, span, LANES), F32),
+        "columns": vmem((3 if folded else 1, span, LANES), F32),
         "mdrec": vmem((2, mix_rows, width), BF16),
         "load_sem": dma((len(inputs),)),
     }
     if folded:
         scratch |= {
-            "qin": vmem((2, span, head_width), BF16),
-            "obuf": vmem((2, head_width, span), BF16),
-            "lbuf": vmem((2, 8, span), F32),
+            "qin": vmem((span, head_width), BF16),
+            "obuf": vmem((head_width, span), BF16),
+            "lbuf": vmem((8, span), F32),
             "oin": vmem((head_width, span), BF16),
             "lin": vmem((8, span), F32),
             "qs": dma((1,)),
-            "qr": dma((2,)),
-            "os": dma((2, 2)),
+            "qr": dma((1,)),
+            "os": dma((2,)),
             "or": dma((2,)),
         }
     scratch |= {"ns": dma((3,)), "nr": dma((3,)), "ms": dma((3,)), "mr": dma((3,))}
@@ -649,7 +709,7 @@
         kernel(n_ep, head_dim, dict(zip(labels, refs, strict=True)))
 
     block = pl.BlockSpec(memory_space=pltpu.VMEM)
-    return pl.pallas_call(
+    results = pl.pallas_call(
         body,
         out_shape=(
             jax.ShapeDtypeStruct((mix_rows, width), BF16),
@@ -662,6 +722,14 @@
             collective_id=0, has_side_effects=True, vmem_limit_bytes=66_500_000
         ),
     )(*inputs.values())
+    anywhere = pl.BlockSpec(memory_space=pl.ANY)
+    return pl.pallas_call(
+        hand_out,
+        out_shape=tuple(jax.ShapeDtypeStruct(x.shape, x.dtype) for x in results),
+        in_specs=[anywhere] * 2,
+        out_specs=(anywhere,) * 2,
+        scratch_shapes=[vmem(x.shape, x.dtype) for x in results] + [dma((2, 4))],
+    )(*results)
 
 
 def solution(mesh):

time: 96.6 us -> 89.2 us (0.923); the launches traced: 94.7 us -> 89.1 us
  local copies, waits for them, and re-layouts: 3.76 us -> 0 us
  Pallas kernels: 90.3 us -> 88.3 us
    pallas_call x1, Pallas kernels: 90.3 us -> 86.3 us  [on_device(): pl.pallas_call(body, out_shape=(jax.ShapeDtypeStruct((mix_rows, width), B...]
    unnamed x2 -> x0, local copies, waits for them, and re-layouts: 3.76 us -> none
    pallas_call x0 -> x1, Pallas kernels: none -> 1.98 us  [on_device(): pl.pallas_call(hand_out, out_shape=tuple((jax.ShapeDtypeStruct(x.shape, x...]
where the time goes in v2:
time: 89.2 us; the launch traced here: 89.1 us
  Pallas kernels  88.3 us (99%)
    pallas_call x1, Pallas kernels, on_device(): pl.pallas_call(body, out_shape=(jax.ShapeDtypeStruct((mix_rows, width), B...  86.3 us
    pallas_call x1, Pallas kernels, on_device(): pl.pallas_call(hand_out, out_shape=tuple((jax.ShapeDtypeStruct(x.shape, x...  1.98 us

profile of v2, /device:TPU:0, one launch (start us, length us, event | category | flops | bytes accessed | tf_op | source)
XLA Modules:
  0.0 89.1 jit_solution(3494571814266529307)
XLA Ops:
  0.6 86.3 %shard_map.158 = (bf16[128,2048]{1,0:T(8,128)(2,1)}, bf16[128,2048]{1,0:T(8,128)(2,1)}) custom-call(bf16[128,2048]{1,0:T(8,128)(2,1)} %refs_0_.1, f32[1,2048]{1,0:T(1,128)} %bitcast.11, s32[2,128]{1,0:T(2,128)} %bitcast.14, bf16[128,2048]{1,0:T(8,128)(2,1)} %refs_3_.1, f32[1,2048]{1,0:T(1,128)} %bitcast.12, bf16[2048,256]{1,0:T(8,128)(2,1)} %refs_5_.1, ...), custom_call_target="tpu_custom_call" | custom-call | tf_op jit(solution)/shard_map/pallas_call | solution.py:712
  86.9 2.0 %shard_map.159 = (bf16[128,2048]{1,0:T(8,128)(2,1)}, bf16[128,2048]{1,0:T(8,128)(2,1)}) custom-call(bf16[128,2048]{1,0:T(8,128)(2,1)} %get-tuple-element.4.refs_0_, bf16[128,2048]{1,0:T(8,128)(2,1)} %get-tuple-element.5.refs_1_), custom_call_target="tpu_custom_call" | custom-call | tf_op jit(solution)/shard_map/pallas_call | solution.py:726

commit v3 on v2

--- a/solution.py
+++ b/solution.py
@@ -391,7 +391,10 @@
 
         relay_c(p1)
         expert_other(p1)
-        step_e(p1)
+
+        @pl.when(jnp.logical_not(last))
+        def _():
+            step_e(p1)
 
         @pl.when(edge)
         def _():
@@ -434,7 +437,13 @@
         def _():
             step_e(me)
 
-        step_f(p1, False)
+        @pl.when(last)
+        def _():
+            step_e(p1)
+
+        @pl.when(jnp.logical_not(last))
+        def _():
+            step_f(p1, False)
 
         @pl.when(helper)
         def _():
@@ -448,7 +457,9 @@
             copy_l.start()
             attend(queries, 2, 0, columns.at[2], 0, False, False)
 
-        step_f(p2, False)
+        @pl.when(jnp.logical_not(helper))
+        def _():
+            step_f(p2, False)
 
         @pl.when(jnp.logical_not(last))
         def _():
@@ -456,6 +467,7 @@
 
         @pl.when(last)
         def _():
+            step_f(p3, False)
             copy_o.wait_recv()
             copy_l.wait_recv()
             for h in range(heads):
@@ -467,8 +479,17 @@
                 attended[:, hc] = (numer / (run_sum[0, h : h + 1] * fix + far_fix)).T.astype(BF16)
 
         mix_out()
-        step_f(p3, False)
+
+        step_f(jnp.where(last, p1, p3), False)
+
+        @pl.when(helper)
+        def _():
+            copy_o.wait_send()
+            copy_l.wait_send()
+            step_f(p2, False)
+
         step_f(me, True)
+
         combine(me, True)
         for e in (p1, p2, p3):
             recv_f(e).wait_recv()
@@ -484,11 +505,6 @@
         def _():
             copy_kv(1, 2).wait_send()
             copy_kv(0, 2).wait_send()
-
-        @pl.when(helper)
-        def _():
-            copy_o.wait_send()
-            copy_l.wait_send()
 
         @pl.when(last)
         def _():

time: 89.2 us -> 88.1 us (0.988); the launches traced: 89.1 us -> 86.5 us
  Pallas kernels: 88.3 us -> 85.7 us
    pallas_call x1, Pallas kernels: 86.3 us -> 83.7 us  [on_device(): pl.pallas_call(body, out_shape=(jax.ShapeDtypeStruct((mix_rows, width), B...]
where the time goes in v3:
time: 88.1 us; the launch traced here: 86.5 us
  Pallas kernels  85.7 us (97%)
    pallas_call x1, Pallas kernels, on_device(): pl.pallas_call(body, out_shape=(jax.ShapeDtypeStruct((mix_rows, width), B...  83.7 us
    pallas_call x1, Pallas kernels, on_device(): pl.pallas_call(hand_out, out_shape=tuple((jax.ShapeDtypeStruct(x.shape, x...  1.98 us

profile of v3, /device:TPU:0, one launch (start us, length us, event | category | flops | bytes accessed | tf_op | source)
XLA Modules:
  0.0 86.5 jit_solution(8608881780229449858)
XLA Ops:
  0.6 83.7 %shard_map.158 = (bf16[128,2048]{1,0:T(8,128)(2,1)}, bf16[128,2048]{1,0:T(8,128)(2,1)}) custom-call(bf16[128,2048]{1,0:T(8,128)(2,1)} %refs_0_.1, f32[1,2048]{1,0:T(1,128)} %bitcast.11, s32[2,128]{1,0:T(2,128)} %bitcast.14, bf16[128,2048]{1,0:T(8,128)(2,1)} %refs_3_.1, f32[1,2048]{1,0:T(1,128)} %bitcast.12, bf16[2048,256]{1,0:T(8,128)(2,1)} %refs_5_.1, ...), custom_call_target="tpu_custom_call" | custom-call | tf_op jit(solution)/shard_map/pallas_call | solution.py:728
  84.3 2.0 %shard_map.159 = (bf16[128,2048]{1,0:T(8,128)(2,1)}, bf16[128,2048]{1,0:T(8,128)(2,1)}) custom-call(bf16[128,2048]{1,0:T(8,128)(2,1)} %get-tuple-element.4.refs_0_, bf16[128,2048]{1,0:T(8,128)(2,1)} %get-tuple-element.5.refs_1_), custom_call_target="tpu_custom_call" | custom-call | tf_op jit(solution)/shard_map/pallas_call | solution.py:742
